TPU v7x, 512 devices: a whole 4x4x16 slice. The times are simulated.
512 devices in a mesh: sp: 32 (over z, core), tp: 16 (over y, x).
Axes of the slice: x: 4, y: 4, z: 16, core: 2. Of those that a mesh axis runs over, the one named last changes fastest.
Arguments:
- outer_gate: bfloat16 [8192, 1024], P('sp', 'tp'), may hold values from -6 to 6
- inner_gate: bfloat16 [8192, 1024], P('sp', 'tp'), may hold values from -6 to 6
- values: bfloat16 [8192, 1024], P('sp', 'tp'), may hold values from -6 to 6
- conv_taps: bfloat16 [3, 1024], P(None, 'tp'), may hold values from -3.5 to 3.5
- document: int32 [8192], P('sp'), may hold values from 0 to 15, never falling along the last dimension, each value on 1 to 1024 neighbouring positions
- mix_proj: bfloat16 [1024, 2048], P('tp'), may hold values from -0.1875 to 0.1875
- stream: bfloat16 [8192, 2048], P('sp'), may hold values from -6 to 6
- norm_gain: float32 [2048], replicated, may hold values from 0.1 to 1.9
- routes: int32 [8192, 2], P('sp'), may hold values from 0 to 31, all different within a row; in each aligned block of 256 rows (0 to 255, 256 to 511, ...) at most 24 rows name the same one
- route_weight: float32 [8192, 2], P('sp'), may hold values from 0.25 to 1
- w_gate: bfloat16 [32, 2048, 4096], P('sp', None, 'tp'), may hold values from -0.125 to 0.125
- w_up: bfloat16 [32, 2048, 4096], P('sp', None, 'tp'), may hold values from -0.125 to 0.125
- w_down: bfloat16 [32, 4096, 2048], P('sp', 'tp'), may hold values from -0.09375 to 0.09375
Outputs:
- mixed: bfloat16 [8192, 2048], P('sp', 'tp')
Inputs may be any that keep to these rules, and one draw needn't show every extreme that they name: Document numbers never fall along the sequence; each document holds 1 to 1024 consecutive tokens and one holds exactly that many. `routes`: each token names 2 different experts. Among the 256 tokens of one sp index no expert is named by more than 24 tokens, and in some sp index's tokens an expert is named by exactly 24.
All inputs are finite; a program needn't handle non-finite values.
Results may differ from a plain program's by a relative error of at most 0.014.
Values may be sent and summed in bfloat16 or wider, within the bound.
A program may use at most 64 MiB of HBM per device.

v0:
```python
import jax
import jax.numpy as jnp
from jax import lax
from jax.sharding import Mesh
from jax.sharding import PartitionSpec as P

TP = ("tp_0", "tp_1")


def in_blocks(x, dim, count):
    before, after = (x.shape[:dim], x.shape[dim + 1 :])
    return jnp.moveaxis(x.reshape(*before, count, -1, *after), dim, 0)


def sum_at_owner(x, axis, dim):
    parts = in_blocks(x, dim, lax.axis_size(axis))
    arrived = lax.all_to_all(parts, axis, split_axis=0, concat_axis=0, tiled=True)
    return arrived.astype(jnp.float32).sum(axis=0)


def passed_along(value, axis, steps):
    count = lax.axis_size(axis)
    first, last = (max(0, -steps), min(count, count - steps))
    return lax.ppermute(value, axis, [(source, source + steps) for source in range(first, last)])


def sent_to_all(x, axis):
    count = lax.axis_size(axis)
    return lax.all_to_all(jnp.broadcast_to(x[None], (count, *x.shape)), axis, 0, 0, tiled=True)


def of_everyone(x, axis):
    everything = sent_to_all(x, axis)
    return jnp.sum(everything, axis=0)


def whole_of(x, axes, dim):
    for axis in reversed(axes):
        x = lax.all_gather(x, axis, axis=dim, tiled=True)
    return x


def finish(gate, upper, w_down):
    act = (jax.nn.silu(gate) * upper).astype(jnp.bfloat16)
    partial_value = jnp.dot(act, w_down[0], preferred_element_type=jnp.float32)
    return sum_at_owner(partial_value.astype(jnp.bfloat16), TP, 1).astype(jnp.bfloat16)


def body(
    outer_gate,
    inner_gate,
    values,
    conv_taps,
    document,
    mix_proj,
    stream,
    norm_gain,
    routes,
    route_weight,
    w_gate,
    w_up,
    w_down,
):
    length = stream.shape[0]
    features = stream.shape[1]
    groups = lax.axis_size("sp")
    capacity = 3 * length // groups
    chosen_count = routes.shape[1]
    width = features // lax.axis_size(TP)
    column = lax.axis_index(TP) * width
    product = inner_gate.astype(jnp.float32) * values.astype(jnp.float32)
    doc_float = document.astype(jnp.float32)
    rim_values, rim_docs = passed_along((product[-2:], doc_float[-2:]), "sp", 1)
    padded_values = jnp.concatenate([rim_values, product], axis=0)
    padded_docs = jnp.concatenate([rim_docs, doc_float], axis=0)
    kernel = conv_taps.astype(jnp.float32)
    conv = kernel[2] * product
    for back in (1, 2):
        offset = 2 - back
        same = (padded_docs[offset : offset + length] == doc_float)[:, None]
        conv = conv + kernel[offset] * jnp.where(same, padded_values[offset : offset + length], 0.0)
    gated = (outer_gate.astype(jnp.float32) * conv).astype(jnp.bfloat16)
    partial_value = jnp.dot(gated, mix_proj, preferred_element_type=jnp.float32)
    gain_part = lax.dynamic_slice_in_dim(norm_gain, column, width, 0)
    own_stream = lax.dynamic_slice_in_dim(stream, column, width, 1).astype(jnp.float32)
    own_part = own_stream + sum_at_owner(partial_value.astype(jnp.bfloat16), TP, 1)
    squares = of_everyone(jnp.sum(own_part * own_part, axis=1), TP)
    scale = lax.rsqrt(squares / features + 1e-06)[:, None]
    normed_part = (own_part * scale * gain_part).astype(jnp.bfloat16)
    flat_expert = routes.reshape(-1)
    picks = (flat_expert[:, None] == jnp.arange(groups, dtype=jnp.int32)[None, :]).astype(jnp.int32)
    ranking = jnp.sum((jnp.cumsum(picks, axis=0) - 1) * picks, axis=1)
    target = flat_expert * capacity + ranking
    token_of = jnp.arange(length * chosen_count, dtype=jnp.int32) // chosen_count
    slot_token = jnp.zeros((groups * capacity,), jnp.int32).at[target].set(token_of + 1)
    filled = (slot_token > 0)[:, None]
    source_row = jnp.maximum(slot_token - 1, 0)
    nothing = jnp.zeros((), jnp.bfloat16)
    outgoing = jnp.where(filled, jnp.take(normed_part, source_row, axis=0), nothing).reshape(
        groups, capacity, width
    )
    arrived = lax.all_to_all(outgoing, "sp", split_axis=0, concat_axis=0, tiled=True)
    piece = whole_of(arrived, TP, 2)
    span = piece.shape[2]
    flat = piece.reshape(-1, span)
    gate_rows = w_gate[0]
    up_rows = w_up[0]
    gate = jnp.dot(flat, gate_rows, preferred_element_type=jnp.float32)
    upper = jnp.dot(flat, up_rows, preferred_element_type=jnp.float32)
    returned = finish(gate, upper, w_down).reshape(groups, capacity, width)
    landed = lax.all_to_all(returned, "sp", split_axis=0, concat_axis=0, tiled=True)
    flat_back = landed.reshape(groups * capacity, width)
    fetched = (
        jnp.take(flat_back, target, axis=0).astype(jnp.float32).reshape(length, chosen_count, width)
    )
    weighted = jnp.sum(fetched * route_weight[:, :, None], axis=1)
    return (own_part + weighted).astype(jnp.bfloat16)


def solution(mesh):
    finer = Mesh(mesh.devices.reshape(mesh.shape["sp"], 4, 4), ("sp", "tp_0", "tp_1"))
    placed = (
        P("sp", TP),
        P("sp", TP),
        P("sp", TP),
        P(None, TP),
        P("sp"),
        P(TP, None),
        P("sp", None),
        P(),
        P("sp", None),
        P("sp", None),
        P("sp", None, TP),
        P("sp", None, TP),
        P("sp", TP, None),
    )
    return jax.shard_map(body, mesh=finer, in_specs=placed, out_specs=P("sp", TP), check_vma=False)
```

profile of v0, /device:TPU:1, one launch (start us, length us, event | category | flops | bytes accessed | tf_op | source)
XLA Modules:
  0.0 254.5 jit_solution(13687493990397626902)
XLA Ops:
  6.5 0.0 copy-start
  6.5 0.8 convert_element_type.55
  7.3 0.1 slice.35
  7.4 4.9 %collective-permute-start = (f32[2]{0:T(128)S(1)}, f32[2]{0:T(128)S(1)}, u32[]{:S(2)}, u32[]{:S(2)}) collective-permute-start(f32[2]{0:T(128)S(1)} %slice.35), channel_id=1, source_target_pairs={{0,16},{16,32},{32,48},{48,64},{64,80},{80,96},{96,112},{112,128},... | collective-permute-start | bytes 32 | tf_op jit(solution)/shard_map/ppermute | solution.py:24
  12.3 0.8 convert_multiply_fusion
  13.1 0.1 slice.48
  13.2 1.9 collective-permute-start.1
  15.1 0.8 copy.44
  15.9 0.1 eq.34
  16.1 0.1 reshape.113
  16.2 0.7 broadcast_multiply_fusion
  16.9 0.7 convert_element_type.52
  17.6 1.2 reduce-window.6
  18.8 0.0 collective-permute-done
  18.8 0.1 pad_maximum_fusion.1
  18.8 0.8 slice_compare_fusion.1
  19.6 0.0 collective-permute-done.1
  19.6 1.5 fusion.1
  21.1 1.3 copy.61
  22.4 6.8 %all-to-all-start = ((bf16[16,256,128]{2,1,0:T(8,128)(2,1)}), bf16[16,256,128]{2,1,0:T(8,128)(2,1)S(1)}, u32[]{:S(2)}, u32[]{:S(2)}) async-start(bf16[16,256,128]{2,1,0:T(8,128)(2,1)} %bitcast.57), calls=%async_computation | async-start | bytes 2097152 | tf_op jit(solution)/shard_map/all_to_all | solution.py:17
  29.2 0.2 slice_reduce_fusion
  29.4 0.1 copy.49
  29.6 0.0 copy-start.3
  29.6 0.1 mul.114
  29.7 0.1 fusion.18
  29.8 2.4 scatter_custom_fusion
  32.3 13.1 %all-to-all-done = bf16[16,256,128]{2,1,0:T(8,128)(2,1)S(1)} async-done(((bf16[16,256,128]{2,1,0:T(8,128)(2,1)}), bf16[16,256,128]{2,1,0:T(8,128)(2,1)S(1)}, u32[]{:S(2)}, u32[]{:S(2)}) %all-to-all-start) | async-done | bytes 1048608 | tf_op jit(solution)/shard_map/all_to_all | solution.py:17
  45.4 0.1 convert_reduce_fusion
  45.5 1.0 multiply_reduce_fusion.1
  46.5 0.6 broadcast_in_dim.78
  47.1 4.5 %all-to-all-start.1 = ((f32[16,1,256]{2,1,0:T(1,128)}), f32[16,1,256]{2,1,0:T(1,128)S(1)}, u32[]{:S(2)}, u32[]{:S(2)}) async-start(f32[16,1,256]{2,1,0:T(1,128)} %broadcast_in_dim.78), calls=%async_computation.1 | async-start | bytes 32768 | tf_op jit(solution)/shard_map/all_to_all | solution.py:29
  51.7 0.0 all-gather.2.cloned.1.call-start
  51.7 0.8 dynamic_slice.7
  52.5 0.1 broadcast_in_dim.74
  52.6 0.1 broadcast_in_dim.76
  52.7 5.4 %all-to-all-done.1 = f32[16,1,256]{2,1,0:T(1,128)S(1)} async-done(((f32[16,1,256]{2,1,0:T(1,128)}), f32[16,1,256]{2,1,0:T(1,128)S(1)}, u32[]{:S(2)}, u32[]{:S(2)}) %all-to-all-start.1) | async-done | bytes 16416 | tf_op jit(solution)/shard_map/all_to_all | solution.py:29
  58.1 0.9 multiply_convert_fusion
  59.1 1.9 gather_fusion
  61.0 0.3 select_select_fusion
  61.3 35.3 %all_to_all.26 = bf16[32,24,128]{2,1,0:T(8,128)(2,1)S(1)} all-to-all(bf16[32,24,128]{2,1,0:T(8,128)(2,1)S(1)} %select_select_fusion), channel_id=1, replica_groups=mesh['sp'=32,'tp_0'=4,'tp_1'=4] {'sp'}, dimensions={0} | all-to-all | bytes 393216 | tf_op jit(solution)/shard_map/all_to_all | solution.py:102
  96.6 15.4 %all_gather.6 = bf16[32,24,512]{2,1,0:T(8,128)(2,1)} all-gather(bf16[32,24,128]{2,1,0:T(8,128)(2,1)S(1)} %all_to_all.26), channel_id=1, replica_groups=mesh['sp'=32,'tp_0'=4,'tp_1'=4] {'tp_1'}, dimensions={2}, use_global_device_ids=true | all-gather | bytes 983040 | tf_op jit(solution)/shard_map/all_gather | solution.py:39
  112.0 0.0 copy-start.4
  112.0 0.0 all-gather.2.cloned.1.call-update
  112.0 37.7 %all-gather.2.cloned.1.call-done = bf16[32,24,2048]{2,1,0:T(8,128)(2,1)} async-done(((bf16[32,24,512]{2,1,0:T(8,128)(2,1)}), bf16[32,24,2048]{2,1,0:T(8,128)(2,1)}) %all-gather.2.cloned.1.call-update) | async-done | bytes 3145744 | tf_op jit(solution)/shard_map/all_gather | solution.py:39
  149.7 0.0 copy-done.3
  149.7 3.8 %fusion.5 = f32[768,256]{1,0:T(8,128)} fusion(bf16[768,2048]{1,0:T(8,128)(2,1)} %bitcast.65, bf16[1,2048,256]{2,1,0:T(8,128)(2,1)S(1)} %copy-done.3), kind=kOutput, calls=%fused_computation.14 | convolution fusion | flops 805306368 | bytes 4980736 | tf_op jit(solution)/shard_map/dot_general | solution.py:108
  153.5 0.0 copy-done
  153.5 0.0 copy-done.4
  153.5 7.1 %fusion = bf16[96,16,8,128]{3,2,1,0:T(8,128)(2,1)} fusion(bf16[1,256,2048]{2,1,0:T(8,128)(2,1)S(1)} %copy-done, bf16[768,2048]{1,0:T(8,128)(2,1)} %bitcast.66, bf16[1,2048,256]{2,1,0:T(8,128)(2,1)S(1)} %copy-done.4, f32[768,256]{1,0:T(8,128)} %fusion.5), kind=kOutput, calls=%fused_computation.7 | convolution fusion | flops 1613365248 | bytes 9175040 | tf_op jit(solution)/shard_map/dot_general | solution.py:45
  160.6 2.7 %copy.60 = bf16[96,16,8,128]{3,2,0,1:T(8,128)(2,1)S(1)} copy(bf16[96,16,8,128]{3,2,1,0:T(8,128)(2,1)} %fusion) | data formatting | bytes 6291456 | tf_op jit(solution)/shard_map/reshape | solution.py:12
  163.3 44.0 %all_to_all.27 = bf16[16,768,128]{2,1,0:T(8,128)(2,1)} all-to-all(bf16[16,768,128]{2,1,0:T(8,128)(2,1)S(1)} %bitcast.58), channel_id=1, replica_groups=mesh['sp'=32,'tp_0'=4,'tp_1'=4] {'tp_0','tp_1'}, dimensions={0} | all-to-all | bytes 6291456 | tf_op jit(solution)/shard_map/all_to_all | solution.py:17
  207.3 0.0 copy-start.1
  207.3 3.1 %reduce_sum.67 = bf16[768,128]{1,0:T(8,128)(2,1)} reduce(bf16[16,768,128]{2,1,0:T(8,128)(2,1)} %all_to_all.27, bf16[]{:T(256)} %constant.85.clone.1), dimensions={0}, to_apply=%region_7.8 | reduce | flops 1474560 | bytes 3342338 | tf_op jit(solution)/shard_map/reduce_sum | solution.py:18
  210.3 14.3 %all-to-all-start.4 = ((bf16[32,24,128]{2,1,0:T(8,128)(2,1)}), bf16[32,24,128]{2,1,0:T(8,128)(2,1)S(1)}, u32[]{:S(2)}, u32[]{:S(2)}) async-start(bf16[32,24,128]{2,1,0:T(8,128)(2,1)} %bitcast.13), calls=%async_computation.4 | async-start | bytes 393216 | tf_op jit(solution)/shard_map/all_to_all | solution.py:111
  224.6 0.1 reduce_sum.63
  224.8 0.1 copy.47
  224.8 0.0 copy-done.1
  224.9 0.2 copy.48
  225.0 0.0 copy-done.2
  225.0 0.1 copy.52
  225.2 18.2 %all-to-all-done.4 = bf16[32,24,128]{2,1,0:T(8,128)(2,1)S(1)} async-done(((bf16[32,24,128]{2,1,0:T(8,128)(2,1)}), bf16[32,24,128]{2,1,0:T(8,128)(2,1)S(1)}, u32[]{:S(2)}, u32[]{:S(2)}) %all-to-all-start.4) | async-done | bytes 196640 | tf_op jit(solution)/shard_map/all_to_all | solution.py:111
  243.4 1.3 gather_fusion.1
  244.7 1.5 multiply_reduce_fusion
  246.2 1.5 add_convert_fusion
  (14 shorter events, 0.2 us)
Async XLA Ops:
  6.5 146.9 %copy-start = (bf16[1,256,2048]{2,1,0:T(8,128)(2,1)S(1)}, bf16[1,256,2048]{2,1,0:T(8,128)(2,1)}, u32[]{:S(2)}) copy-start(bf16[1,256,2048]{2,1,0:T(8,128)(2,1)} %param.25) | copy-start | bytes 3145732
  7.4 11.4 %collective-permute-start = (f32[2]{0:T(128)S(1)}, f32[2]{0:T(128)S(1)}, u32[]{:S(2)}, u32[]{:S(2)}) collective-permute-start(f32[2]{0:T(128)S(1)} %slice.35), channel_id=1, source_target_pairs={{0,16},{16,32},{32,48},{48,64},{64,80},{80,96},{96,112},{112,128},... | collective-permute-start | bytes 32 | tf_op jit(solution)/shard_map/ppermute | solution.py:24
  13.2 6.4 %collective-permute-start.1 = (f32[2,64]{0,1:T(8,128)S(1)}, f32[2,64]{0,1:T(8,128)S(1)}, u32[]{:S(2)}, u32[]{:S(2)}) collective-permute-start(f32[2,64]{0,1:T(8,128)S(1)} %slice.48), channel_id=1, source_target_pairs={{0,16},{16,32},{32,48},{48,64},{64,80},{80,96},{96,112},{112,128},... | collective-permute-start | bytes 1544 | tf_op jit(solution)/shard_map/ppermute | solution.py:24
  22.4 23.0 %all-to-all-start = ((bf16[16,256,128]{2,1,0:T(8,128)(2,1)}), bf16[16,256,128]{2,1,0:T(8,128)(2,1)S(1)}, u32[]{:S(2)}, u32[]{:S(2)}) async-start(bf16[16,256,128]{2,1,0:T(8,128)(2,1)} %bitcast.57), calls=%async_computation | async-start | bytes 2097152 | tf_op jit(solution)/shard_map/all_to_all | solution.py:17
  29.6 120.1 %copy-start.3 = (bf16[1,2048,256]{2,1,0:T(8,128)(2,1)S(1)}, bf16[1,2048,256]{2,1,0:T(8,128)(2,1)}, u32[]{:S(2)}) copy-start(bf16[1,2048,256]{2,1,0:T(8,128)(2,1)} %param.23) | copy-start | bytes 3145732
  47.1 11.0 %all-to-all-start.1 = ((f32[16,1,256]{2,1,0:T(1,128)}), f32[16,1,256]{2,1,0:T(1,128)S(1)}, u32[]{:S(2)}, u32[]{:S(2)}) async-start(f32[16,1,256]{2,1,0:T(1,128)} %broadcast_in_dim.78), calls=%async_computation.1 | async-start | bytes 32768 | tf_op jit(solution)/shard_map/all_to_all | solution.py:29
  51.7 98.0 %all-gather.2.cloned.1.call-start = ((), (), s32[]{:S(2)}) async-start(), calls=%async_computation.5 | async-start | bytes 3932160 | tf_op jit(solution)/shard_map/all_gather | solution.py:39
  112.0 41.5 %copy-start.4 = (bf16[1,2048,256]{2,1,0:T(8,128)(2,1)S(1)}, bf16[1,2048,256]{2,1,0:T(8,128)(2,1)}, u32[]{:S(2)}) copy-start(bf16[1,2048,256]{2,1,0:T(8,128)(2,1)} %param.24) | copy-start | bytes 3145732
  207.3 17.6 %copy-start.1 = (s32[256,2]{0,1:T(2,128)S(1)}, s32[256,2]{0,1:T(2,128)}, u32[]{:S(2)}) copy-start(s32[256,2]{0,1:T(2,128)} %param.21) | copy-start | bytes 6148
  207.3 17.8 %copy-start.2 = (f32[256,2]{0,1:T(2,128)S(1)}, f32[256,2]{0,1:T(2,128)}, u32[]{:S(2)}) copy-start(f32[256,2]{0,1:T(2,128)} %param.22) | copy-start | bytes 6148
  210.3 33.1 %all-to-all-start.4 = ((bf16[32,24,128]{2,1,0:T(8,128)(2,1)}), bf16[32,24,128]{2,1,0:T(8,128)(2,1)S(1)}, u32[]{:S(2)}, u32[]{:S(2)}) async-start(bf16[32,24,128]{2,1,0:T(8,128)(2,1)} %bitcast.13), calls=%async_computation.4 | async-start | bytes 393216 | tf_op jit(solution)/shard_map/all_to_all | solution.py:111
Sparse Core Ops, SparseCore 0:
  112.1 37.5 all-gather.1
where the time goes:
time: 255 us
  blocking collectives  94.7 us (37%)
  waiting for transfers between devices  74.4 us (29%)
  starting transfers between devices  32.4 us (13%)
  between operations  13.6 us (5%)
  local copies, waits for them, and re-layouts  13.5 us (5%)
  other arithmetic  13.5 us (5%)
  matrix products  12.4 us (5%)
    all_to_all x1, blocking collectives, sum_at_owner(): lax.all_to_all(parts, axis, split_axis=0, concat_axis=0, tiled=True)  44 us
    all_gather x1, waiting for transfers between devices, whole_of(): x = lax.all_gather(x, axis, axis=dim, tiled=True)  37.7 us
    all_to_all x1, blocking collectives, body(): lax.all_to_all(outgoing, 'sp', split_axis=0, concat_axis=0, tiled=True)  35.3 us
    all_to_all x1, waiting for transfers between devices, body(): lax.all_to_all(returned, 'sp', split_axis=0, concat_axis=0, tiled=True)  18.2 us
    all_gather x1, blocking collectives, whole_of(): x = lax.all_gather(x, axis, axis=dim, tiled=True)  15.4 us
    all_to_all x1, starting transfers between devices, body(): lax.all_to_all(returned, 'sp', split_axis=0, concat_axis=0, tiled=True)  14.3 us
    all_to_all x1, waiting for transfers between devices, sum_at_owner(): lax.all_to_all(parts, axis, split_axis=0, concat_axis=0, tiled=True)  13.1 us
    dot_general x1, matrix products, finish(): partial_value = jnp.dot(act, w_down[0], preferred_element_type=jnp.float32)  7.11 us
  transfers between devices with their start and end apart: 6, of which 4 were waited for; matrix products, arithmetic and copies ran while one was open for 4% of the time, Pallas kernels for 0%

commit v1 on v0

v1 whole, which is shorter than its diff:
```python
import jax
import jax.numpy as jnp
from jax import lax
from jax.experimental import pallas as pl
from jax.experimental.pallas import tpu as pltpu
from jax.sharding import PartitionSpec as P

MESH = pl.DeviceIdType.MESH
F32 = jnp.float32
BF16 = jnp.bfloat16

NZ = 16
NS = 32
CAP = 24
W = 128
CHUNKS = 4
BLOCKS = 8
ROWS = BLOCKS * CAP

ORDER = (0, 1, 15, 2, 14, 3, 13, 4, 12, 5, 11, 6, 10, 7, 9, 8)
PLACE = {r: i for i, r in enumerate(ORDER)}

NT = (((1,), (1,)), ((), ()))


def kernel(
    og_ref, ig_ref, vv_ref, taps_ref, doc_ref, mix_hbm, stream_hbm, gain_ref, routes_ref, rw_ref, wg_hbm, wu_hbm, wd_hbm,
    out_ref,
    mix, stream, wg, wu, wd, hsend, hrecv, mbuf, blk, gbuf, hid, dmat, dt0, dt1, wcol, sent, x_all, lhs, p_all, rb0, rb1, rb2, q_all, f_all, back,
    lsem, hs, hr, ms, mr, gs, gr, zs, zr, as_, ar, rs, rr, bs, br,
):
    s = lax.axis_index("sp")
    t = lax.axis_index("tp")
    z, c = s // 2, s % 2
    y, x = t // 4, t % 4

    def plane(yy, xx):
        return (s, yy * 4 + xx)

    def along_z(r, dc):
        return (z + r + NZ) % NZ * 2 + (c + dc) % 2

    barrier = pltpu.get_barrier_semaphore()
    for d in range(1, 16):
        pl.semaphore_signal(barrier, inc=1, device_id=(s, (t + d) % 16), device_id_type=MESH)
    for d in range(1, NS):
        pl.semaphore_signal(barrier, inc=1, device_id=((s + d) % NS, t), device_id_type=MESH)

    loads = [
        pltpu.make_async_copy(mix_hbm, mix, lsem.at[0]),
        pltpu.make_async_copy(stream_hbm.at[:, pl.ds(pl.multiple_of(t * W, W), W)], stream, lsem.at[1]),
        pltpu.make_async_copy(wg_hbm, wg, lsem.at[2]),
        pltpu.make_async_copy(wu_hbm, wu, lsem.at[3]),
        pltpu.make_async_copy(wd_hbm, wd, lsem.at[4]),
    ]
    for load in loads:
        load.start()

    started = []

    def remote(src, dst, ssem, rsem, device):
        copy = pltpu.make_async_remote_copy(
            src_ref=src, dst_ref=dst, send_sem=ssem, recv_sem=rsem, device_id=device, device_id_type=MESH
        )
        copy.start()
        started.append(copy)
        return copy

    product = ig_ref[...].astype(F32) * vv_ref[...].astype(F32)
    doc = jnp.broadcast_to(doc_ref[...].astype(F32), (8, 256))
    hsend[0:64, :] = product[:, 128:]
    hsend[64:72, :] = doc[:, 128:]
    loads[0].wait()
    pl.semaphore_wait(barrier, 15 + NS - 1)

    halo = remote(hsend, hrecv, hs.at[0], hr.at[0], ((s + 1) % NS, t))
    mixes = []
    for d in range(1, 16):
        j = (t + d) % 16
        mixes.append(
            remote(mix.at[:, pl.ds(pl.multiple_of(j * W, W), W)], mbuf.at[t], ms.at[d], mr.at[d], (s, j))
        )
    mbuf[t] = mix[:, pl.ds(pl.multiple_of(t * W, W), W)]

    eye = (lax.broadcasted_iota(jnp.int32, (64, 64), 0) == lax.broadcasted_iota(jnp.int32, (64, 64), 1)).astype(BF16)
    kernel_taps = lax.dot_general(eye, taps_ref[...], NT, preferred_element_type=F32)

    halo.wait_recv()
    before = hrecv[0:64, :]
    doc_before = jnp.where(s == 0, -1.0, hrecv[64:72, :])
    long = jnp.concatenate([before, product], axis=1)
    long_doc = jnp.concatenate([doc_before, doc], axis=1)
    conv = kernel_taps[:, 2:3] * product
    for step in (1, 2):
        shifted = pltpu.roll(long, step, 1)[:, 128:]
        same = (pltpu.roll(long_doc, step, 1)[:, 128:] == doc)[0:1, :]
        conv = conv + kernel_taps[:, 2 - step : 3 - step] * jnp.where(same, shifted, 0.0)
    gated = og_ref[...].astype(F32) * conv
    folded = jnp.concatenate([gated[:, :128], gated[:, 128:]], axis=0)
    gbuf[t] = folded.T.astype(BF16)
    gathers = []
    for d in range(1, 16):
        gathers.append(remote(gbuf.at[t], gbuf.at[t], gs.at[d], gr.at[d], (s, (t + d) % 16)))

    expert = lax.broadcasted_iota(jnp.int32, (NS, 256), 0)
    first = (routes_ref[0:1, :] == expert).astype(F32)
    second = (routes_ref[1:2, :] == expert).astype(F32)
    used = first + second
    earlier = (lax.broadcasted_iota(jnp.int32, (256, 256), 0) < lax.broadcasted_iota(jnp.int32, (256, 256), 1)).astype(BF16)
    rank = jnp.dot(used.astype(BF16), earlier, preferred_element_type=F32)
    ranked = jnp.where(used > 0.0, rank, -1.0)
    slot = lax.broadcasted_iota(jnp.int32, (CAP, 256), 0).astype(F32)
    for e in range(0, NS, 2):
        pair = [(jnp.broadcast_to(ranked[i : i + 1, :], (CAP, 256)) == slot).astype(F32) for i in (e, e + 1)]
        dmat[e * CAP : (e + 2) * CAP, :] = jnp.concatenate(pair, axis=0).astype(BF16)
    place = expert.astype(F32) * CAP + rank
    rows = [jnp.sum(first * place, axis=0, keepdims=True), jnp.sum(second * place, axis=0, keepdims=True), rw_ref[0:1, :], rw_ref[1:2, :]]
    wcol[...] = jnp.concatenate([*rows, jnp.zeros((124, 256), F32)], axis=0).T
    lane = lax.broadcasted_iota(jnp.int32, (256, NS * CAP), 1).astype(F32)
    dt0[...] = (wcol[:, 0:1] == lane).astype(F32).astype(BF16)
    dt1[...] = (wcol[:, 1:2] == lane).astype(F32).astype(BF16)

    blk[...] = jnp.zeros_like(blk)
    for copy in mixes:
        copy.wait_recv()
    for j in range(16):
        part = mbuf[j]
        blk[128 * j : 128 * j + 64, 0:128] = part
        blk[128 * j + 64 : 128 * j + 128, 128:256] = part
    loads[1].wait()
    for copy in gathers:
        copy.wait_recv()
    branch = jnp.dot(jnp.concatenate([gbuf[j] for j in range(16)], axis=1), blk[...], preferred_element_type=F32)
    hid[0:128, :] = stream[0:128, :].astype(F32) + branch[:, 0:128]
    hid[128:256, :] = stream[128:256, :].astype(F32) + branch[:, 128:256]
    scaled = (hid[...] * gain_ref[pl.ds(t, 1), :]).astype(BF16)
    sent[...] = jnp.dot(dmat[...], scaled, preferred_element_type=F32).reshape(NS, CAP, W).astype(BF16)

    x_all[0, y, x, 0] = sent[s]
    arrivals = {}
    for i, r in enumerate(ORDER):
        for dc in range(2):
            if r == 0 and dc == 0:
                continue
            e = along_z(-r, dc)
            arrivals[2 * i + dc] = remote(
                sent.at[e], x_all.at[i // 4, y, x, i % 4 * 2 + dc], zs.at[2 * i + dc], zr.at[2 * i + dc], (e, t)
            )
    for load in loads[2:]:
        load.wait()

    def span(col, start, size):
        return pl.ds(4 * col + start, size)

    def by_first(col, ref, k, f, start=0, size=4):
        return ref.at[k, :, f, span(col, start, size)] if col == 0 else ref.at[k, f, :, span(col, start, size)]

    def by_second(col, ref, k, g, start=0, size=4):
        fs = pl.ds(start, size)
        return ref.at[k, g, fs, span(col, 0, 4)] if col == 0 else ref.at[k, fs, g, span(col, 0, 4)]

    first_of = (x, y)
    second_of = (y, x)

    def on_first(col, f):
        return plane(y, f) if col == 0 else plane(f, x)

    def on_second(col, g):
        return plane(g, x) if col == 0 else plane(y, g)

    inv_gain = 1.0 / (gain_ref[...] * gain_ref[...])
    pending = {}

    def gather_first(k):
        for b in range(BLOCKS):
            if k or b:
                arrivals[BLOCKS * k + b].wait_recv()
        out = []
        for col in range(2):
            own = x_all.at[k, y, x, span(col, 0, 4)]
            for d in (1, 3, 2):
                i = 3 * col + d - 1
                out.append(remote(own, own, as_.at[k, i], ar.at[k, i], on_first(col, (first_of[col] + d) % 4)))
        pending["first", k] = out

    def gather_second(k):
        for copy in pending["first", k]:
            copy.wait_recv()
        out = []
        for col in range(2):
            g = second_of[col]
            for way, d in enumerate((1, 3)):
                i = 6 + 2 * col + way
                ref = by_second(col, x_all, k, g)
                out.append(remote(ref, ref, as_.at[k, i], ar.at[k, i], on_second(col, (g + d) % 4)))
        pending["second", k] = out

    def gather_third(k):
        for copy in pending["second", k]:
            copy.wait_recv()
        out = []
        for col in range(2):
            g = second_of[col]
            for way, d in enumerate((1, 3)):
                i = 10 + 2 * col + way
                ref = by_second(col, x_all, k, (g + 4 - d) % 4, 2 * way, 2)
                out.append(remote(ref, ref, as_.at[k, i], ar.at[k, i], on_second(col, (g + d) % 4)))
        pending["third", k] = out

    def experts(k):
        for copy in pending["third", k]:
            copy.wait_recv()
        squares = jnp.zeros((ROWS, W), F32)
        for j in range(16):
            part = x_all[k, j // 4, j % 4].astype(F32).reshape(ROWS, W)
            squares = squares + part * part * inv_gain[j : j + 1, :]
            lhs[:, W * j : W * (j + 1)] = part.astype(BF16)
        scale = lax.rsqrt(jnp.sum(squares, axis=1, keepdims=True) / 2048.0 + 1e-06)
        gate = jnp.dot(lhs[...], wg[...], preferred_element_type=F32) * scale
        upper = jnp.dot(lhs[...], wu[...], preferred_element_type=F32) * scale
        act = (gate / (1.0 + jnp.exp(-gate)) * upper).astype(BF16)
        for yy in range(4):
            partial = jnp.dot(act, wd[:, 512 * yy : 512 * (yy + 1)], preferred_element_type=F32)
            for xx in range(4):
                p_all[k, yy, xx] = partial[:, W * xx : W * (xx + 1)].reshape(BLOCKS, CAP, W).astype(BF16)
        out = []
        for col in range(2):
            f = first_of[col]
            for way, d in enumerate((1, 3)):
                i = 2 * col + way
                out.append(
                    remote(
                        by_first(col, p_all, k, (f + 2) % 4, 2 * way, 2), rb0.at[k, col, way],
                        rs.at[k, i], rr.at[k, i], on_first(col, (f + d) % 4),
                    )
                )
        pending["opposite", k] = out

    def reduce_first(k):
        for copy in pending["opposite", k]:
            copy.wait_recv()
        out = []
        for col in range(2):
            f = first_of[col]
            for way, d in enumerate((1, 3)):
                i = 4 + 2 * col + way
                other = (f + d) % 4
                half = by_first(col, p_all, k, other, 2 * way, 2)
                half[...] = (half[...].astype(F32) + rb0[k, col, way].astype(F32)).astype(BF16)
                out.append(
                    remote(by_first(col, p_all, k, other), rb1.at[k, col, way], rs.at[k, i], rr.at[k, i], on_first(col, other))
                )
        pending["nearby", k] = out

    def reduce_second(k):
        for copy in pending["nearby", k]:
            copy.wait_recv()
        out = []
        for col in range(2):
            f, g = first_of[col], second_of[col]
            total = by_first(col, p_all, k, f)[...].astype(F32) + rb1[k, col, 0].astype(F32) + rb1[k, col, 1].astype(F32)
            q_all[k, col] = total.astype(BF16)
            for d in (1, 3, 2):
                i = 8 + 3 * col + d - 1
                other = (g + d) % 4
                out.append(remote(q_all.at[k, col, other], rb2.at[k, col, d - 1], rs.at[k, i], rr.at[k, i], on_second(col, other)))
        pending["last", k] = out

    returns = []

    def give_back(k):
        for copy in pending["last", k]:
            copy.wait_recv()
        for col in range(2):
            total = q_all[k, col, second_of[col]].astype(F32)
            for d in range(3):
                total = total + rb2[k, col, d].astype(F32)
            f_all[k, 4 * col : 4 * col + 4] = total.astype(BF16)
        for b in range(BLOCKS):
            i = BLOCKS * k + b
            if i == 0:
                back[s] = f_all[0, 0]
                continue
            home = along_z(ORDER[i // 2], i % 2)
            returns.append(remote(f_all.at[k, b], back.at[s], bs.at[i], br.at[i], (home, t)))

    stages = (gather_first, gather_second, gather_third, experts, reduce_first, reduce_second, give_back)
    for step in range(CHUNKS + len(stages) - 1):
        for number, stage in enumerate(stages):
            if 0 <= step - number < CHUNKS:
                stage(step - number)

    for copy in returns:
        copy.wait_recv()
    landed = back[...].astype(F32).reshape(NS * CAP, W).astype(BF16)
    one = jnp.dot(dt0[...], landed, preferred_element_type=F32)
    two = jnp.dot(dt1[...], landed, preferred_element_type=F32)
    out_ref[...] = (hid[...] + (wcol[:, 2:3] * one + wcol[:, 3:4] * two)).astype(BF16)
    for copy in started:
        copy.wait_send()


def body(outer_gate, inner_gate, values, conv_taps, document, mix_proj, stream, norm_gain, routes, route_weight, w_gate, w_up, w_down):
    vmem = pl.BlockSpec(memory_space=pltpu.VMEM)
    hbm = pl.BlockSpec(memory_space=pl.ANY)
    dma = pltpu.SemaphoreType.DMA
    scratch = [
        pltpu.VMEM((64, 2048), BF16),
        pltpu.VMEM((256, W), BF16),
        pltpu.VMEM((2048, 256), BF16),
        pltpu.VMEM((2048, 256), BF16),
        pltpu.VMEM((256, 2048), BF16),
        pltpu.VMEM((72, 128), F32),
        pltpu.VMEM((72, 128), F32),
        pltpu.VMEM((16, 64, W), BF16),
        pltpu.VMEM((2048, 256), BF16),
        pltpu.VMEM((16, 128, 128), BF16),
        pltpu.VMEM((256, W), F32),
        pltpu.VMEM((NS * CAP, 256), BF16),
        pltpu.VMEM((256, NS * CAP), BF16),
        pltpu.VMEM((256, NS * CAP), BF16),
        pltpu.VMEM((256, 128), F32),
        pltpu.VMEM((NS, CAP, W), BF16),
        pltpu.VMEM((CHUNKS, 4, 4, BLOCKS, CAP, W), BF16),
        pltpu.VMEM((ROWS, 2048), BF16),
        pltpu.VMEM((CHUNKS, 4, 4, BLOCKS, CAP, W), BF16),
        pltpu.VMEM((CHUNKS, 2, 2, 4, 2, CAP, W), BF16),
        pltpu.VMEM((CHUNKS, 2, 2, 4, 4, CAP, W), BF16),
        pltpu.VMEM((CHUNKS, 2, 3, 4, CAP, W), BF16),
        pltpu.VMEM((CHUNKS, 2, 4, 4, CAP, W), BF16),
        pltpu.VMEM((CHUNKS, BLOCKS, CAP, W), BF16),
        pltpu.VMEM((NS, CAP, W), BF16),
        dma((5,)),
        dma((1,)), dma((1,)),
        dma((16,)), dma((16,)),
        dma((16,)), dma((16,)),
        dma((NS,)), dma((NS,)),
        dma((CHUNKS, 14)), dma((CHUNKS, 14)),
        dma((CHUNKS, 14)), dma((CHUNKS, 14)),
        dma((NS,)), dma((NS,)),
    ]
    return pl.pallas_call(
        kernel,
        out_shape=jax.ShapeDtypeStruct((256, W), BF16),
        in_specs=[vmem, vmem, vmem, vmem, vmem, hbm, hbm, vmem, vmem, vmem, hbm, hbm, hbm],
        out_specs=vmem,
        scratch_shapes=scratch,
        compiler_params=pltpu.CompilerParams(collective_id=0, has_side_effects=True, vmem_limit_bytes=60 * 2**20),
        name="block",
    )(
        outer_gate.T, inner_gate.T, values.T, conv_taps, document.reshape(1, 256), mix_proj, stream, norm_gain.reshape(16, 128),
        routes.T, route_weight.T, w_gate[0], w_up[0], w_down[0],
    )


def solution(mesh):
    placed = (
        P("sp", "tp"), P("sp", "tp"), P("sp", "tp"), P(None, "tp"), P("sp"), P("tp", None), P("sp", None), P(),
        P("sp", None), P("sp", None), P("sp", None, "tp"), P("sp", None, "tp"), P("sp", "tp", None),
    )
    return jax.shard_map(body, mesh=mesh, in_specs=placed, out_specs=P("sp", "tp"), check_vma=False)
```

time: 255 us -> 90.4 us (0.35)
  blocking collectives: 94.7 us -> 0 us
  Pallas kernels: 0 us -> 88.7 us
  waiting for transfers between devices: 74.4 us -> 0 us
  starting transfers between devices: 32.4 us -> 0 us
  between operations: 13.6 us -> 0.01 us
  other arithmetic: 13.5 us -> 0 us
  matrix products: 12.4 us -> 0 us
  local copies, waits for them, and re-layouts: 13.5 us -> 1.47 us
    pallas_call x0 -> x1, Pallas kernels: none -> 88.7 us  [body(): pl.pallas_call(kernel, out_shape=jax.ShapeDtypeStruct((256, W), BF16), in...]
    all_to_all x2 -> x0, blocking collectives: 79.3 us -> none  [the longest x1 44 us: sum_at_owner(): lax.all_to_all(parts, axis, split_axis=0, concat_axis=0, tiled=True)]
    all_gather x1 -> x0, waiting for transfers between devices: 37.7 us -> none  [whole_of(): x = lax.all_gather(x, axis, axis=dim, tiled=True)]
    all_to_all x3 -> x0, waiting for transfers between devices: 36.7 us -> none  [the longest x1 18.2 us: body(): lax.all_to_all(returned, 'sp', split_axis=0, concat_axis=0, tiled=True)]
    all_to_all x3 -> x0, starting transfers between devices: 25.6 us -> none  [the longest x1 14.3 us: body(): lax.all_to_all(returned, 'sp', split_axis=0, concat_axis=0, tiled=True)]
    all_gather x1 -> x0, blocking collectives: 15.4 us -> none  [whole_of(): x = lax.all_gather(x, axis, axis=dim, tiled=True)]
    dot_general x3 -> x0, matrix products: 12.4 us -> none  [the longest x1 7.11 us: finish(): partial_value = jnp.dot(act, w_down[0], preferred_element_type=jnp.float32)]
    ppermute x2 -> x0, starting transfers between devices: 6.83 us -> none  [passed_along(): lax.ppermute(value, axis, [(source, source + steps) for source in range(f...]
  transfers between devices with their start and end apart: 6 -> 0, of which waited for: 4 -> 0; matrix products, arithmetic and copies ran while one was open for 4% -> 0% of each run, Pallas kernels for 0% -> 0%
where the time goes in v1:
time: 90.4 us; the launch traced here: 90.2 us
  Pallas kernels  88.7 us (98%)
  local copies, waits for them, and re-layouts  1.47 us (2%)
    pallas_call x1, Pallas kernels, body(): pl.pallas_call(kernel, out_shape=jax.ShapeDtypeStruct((256, W), BF16), in...  88.7 us

profile of v1, /device:TPU:1, one launch (start us, length us, event | category | flops | bytes accessed | tf_op | source)
XLA Modules:
  0.0 90.2 jit_solution(7696436195880347837)
XLA Ops:
  0.0 88.7 %block.1 = bf16[256,128]{1,0:T(8,128)(2,1)} custom-call(bf16[64,256]{1,0:T(8,128)(2,1)} %bitcast.13, bf16[64,256]{1,0:T(8,128)(2,1)} %bitcast.14, bf16[64,256]{1,0:T(8,128)(2,1)} %bitcast.15, bf16[3,64]{1,0:T(4,128)(2,1)} %taps_ref.1, s32[1,256]{1,0:T(1,128)} %bitcast.19, bf16[64,2048]{1,0:T(8,128)(2,1)} %mix_hbm.1, bf16[256,2048]{1,0:T(8,128)(2,1)} %stream_hbm.1, ...), custom_call_target="tpu_custom_call" | custom-call | tf_op jit(solution)/shard_map/block/pallas_call | solution.py:342
  88.7 1.5 %copy.15 = bf16[256,128]{1,0:T(8,128)(2,1)} copy(bf16[256,128]{1,0:T(8,128)(2,1)} %block.1) | data formatting | bytes 131072

commit v2 on v1

v2 whole, which is shorter than its diff:
```python
import jax
import jax.numpy as jnp
from jax import lax
from jax.experimental import pallas as pl
from jax.experimental.pallas import tpu as pltpu
from jax.sharding import PartitionSpec as P

MESH = pl.DeviceIdType.MESH
F32 = jnp.float32
BF16 = jnp.bfloat16

NZ = 16
NS = 32
CAP = 24
W = 128
CHUNKS = 8
BLOCKS = NS // CHUNKS
HALF = BLOCKS // 2
PART = HALF // 2
ROWS = BLOCKS * CAP

ORDER = (0, 1, 14, 3, 13, 4, 9, 8, 10, 7, 11, 6, 12, 5, 15, 2)

SCHEDULE = ((0, 0), (0, 1), (0, 2), (1, 0), (1, 1), (1, 2), (0, 3), (2, 0), (0, 4), (0, 7), (0, 5), (2, 1), (2, 2), (0, 6), (1, 3), (1, 4), (1, 5), (1, 7), (2, 3), (3, 2), (2, 4), (1, 6), (2, 5), (3, 1), (2, 7), (3, 3), (4, 2), (3, 4), (2, 6), (3, 0), (3, 5), (3, 7), (4, 3), (4, 4), (3, 6), (4, 7), (5, 3), (4, 5), (5, 4), (4, 6), (4, 1), (5, 5), (4, 0), (6, 3), (6, 4), (5, 6), (5, 2), (5, 7), (5, 1), (6, 5), (5, 0), (6, 6), (6, 2), (6, 1), (6, 7), (6, 0))

NT = (((1,), (1,)), ((), ()))


def kernel(
    og_hbm, ig_hbm, vv_hbm, taps_hbm, doc_hbm, mix_hbm, stream_hbm, gain_hbm, routes_hbm, rw_hbm, wg_hbm, wu_hbm, wd_hbm,
    out_ref,
    gates, taps_ref, doc_ref, gain_ref, routes_ref, rw_ref, mix, stream, wg, wu, wd, hsend, hrecv, mbuf, blk, gbuf, hid, dmat, dt0, dt1, wcol, sent, x_all, lhs, p_all, rb0, rb1, rb2, q_all, f_all, back,
    lsem, hs, hr, ms, mr, gs, gr, zs, zr, ss, sr, bs, br,
):
    s = lax.axis_index("sp")
    t = lax.axis_index("tp")
    z, c = s // 2, s % 2
    y, x = t // 4, t % 4

    def plane(yy, xx):
        return (s, yy * 4 + xx)

    def along_z(r, dc):
        return (z + r + NZ) % NZ * 2 + (c + dc) % 2

    barrier = pltpu.get_barrier_semaphore()
    for d in range(1, 16):
        pl.semaphore_signal(barrier, inc=1, device_id=(s, (t + d) % 16), device_id_type=MESH)
    for d in range(1, NS):
        pl.semaphore_signal(barrier, inc=1, device_id=((s + d) % NS, t), device_id_type=MESH)

    pairs = (
        (ig_hbm, gates.at[0]), (vv_hbm, gates.at[1]), (doc_hbm, doc_ref), (mix_hbm, mix), (og_hbm, gates.at[2]), (taps_hbm, taps_ref),
        (routes_hbm, routes_ref), (rw_hbm, rw_ref), (gain_hbm, gain_ref),
        (stream_hbm.at[:, pl.ds(pl.multiple_of(t * W, W), W)], stream), (wg_hbm, wg), (wu_hbm, wu), (wd_hbm, wd),
    )
    loads = [pltpu.make_async_copy(src, dst, lsem.at[i]) for i, (src, dst) in enumerate(pairs)]
    for load in loads:
        load.start()

    def wait_for(ref, sem):
        pltpu.make_async_copy(ref, ref, sem).wait()

    def remote(src, dst, ssem, rsem, device):
        copy = pltpu.make_async_remote_copy(
            src_ref=src, dst_ref=dst, send_sem=ssem, recv_sem=rsem, device_id=device, device_id_type=MESH
        )
        copy.start()

    for load in loads[:3]:
        load.wait()
    product = gates[0].astype(F32) * gates[1].astype(F32)
    doc = jnp.broadcast_to(doc_ref[...].astype(F32), (8, 256))
    hsend[0:64, :] = product[:, 128:]
    hsend[64:72, :] = doc[:, 128:]
    loads[3].wait()
    pl.semaphore_wait(barrier, 15 + NS - 1)

    remote(hsend, hrecv, hs.at[0], hr.at[0], ((s + 1) % NS, t))
    for d in range(1, 16):
        j = (t + d) % 16
        remote(mix.at[:, pl.ds(pl.multiple_of(j * W, W), W)], mbuf.at[t], ms.at[0], mr.at[0], (s, j))
    mbuf[t] = mix[:, pl.ds(pl.multiple_of(t * W, W), W)]

    eye = (lax.broadcasted_iota(jnp.int32, (64, 64), 0) == lax.broadcasted_iota(jnp.int32, (64, 64), 1)).astype(BF16)
    for load in loads[4:]:
        load.wait()
    kernel_taps = lax.dot_general(eye, taps_ref[...], NT, preferred_element_type=F32)

    wait_for(hrecv, hr.at[0])
    before = hrecv[0:64, :]
    doc_before = jnp.where(s == 0, -1.0, hrecv[64:72, :])
    long = jnp.concatenate([before, product], axis=1)
    long_doc = jnp.concatenate([doc_before, doc], axis=1)
    conv = kernel_taps[:, 2:3] * product
    for step in (1, 2):
        shifted = pltpu.roll(long, step, 1)[:, 128:]
        same = (pltpu.roll(long_doc, step, 1)[:, 128:] == doc)[0:1, :]
        conv = conv + kernel_taps[:, 2 - step : 3 - step] * jnp.where(same, shifted, 0.0)
    gated = gates[2].astype(F32) * conv
    folded = jnp.concatenate([gated[:, :128], gated[:, 128:]], axis=0)
    gbuf[t] = folded.T.astype(BF16)
    for d in range(1, 16):
        remote(gbuf.at[t], gbuf.at[t], gs.at[0], gr.at[0], (s, (t + d) % 16))

    expert = lax.broadcasted_iota(jnp.int32, (NS, 256), 0)
    first = (routes_ref[0:1, :] == expert).astype(F32)
    second = (routes_ref[1:2, :] == expert).astype(F32)
    used = first + second
    earlier = (lax.broadcasted_iota(jnp.int32, (256, 256), 0) < lax.broadcasted_iota(jnp.int32, (256, 256), 1)).astype(BF16)
    rank = jnp.dot(used.astype(BF16), earlier, preferred_element_type=F32)
    ranked = jnp.where(used > 0.0, rank, -1.0)
    slot = lax.broadcasted_iota(jnp.int32, (CAP, 256), 0).astype(F32)
    for e in range(0, NS, 2):
        pair = [(jnp.broadcast_to(ranked[i : i + 1, :], (CAP, 256)) == slot).astype(F32) for i in (e, e + 1)]
        dmat[e * CAP : (e + 2) * CAP, :] = jnp.concatenate(pair, axis=0).astype(BF16)
    place = expert.astype(F32) * CAP + rank
    rows = [jnp.sum(first * place, axis=0, keepdims=True), jnp.sum(second * place, axis=0, keepdims=True), rw_ref[0:1, :], rw_ref[1:2, :]]
    wcol[...] = jnp.concatenate([*rows, jnp.zeros((124, 256), F32)], axis=0).T
    lane = lax.broadcasted_iota(jnp.int32, (256, NS * CAP), 1).astype(F32)
    dt0[...] = (wcol[:, 0:1] == lane).astype(F32).astype(BF16)
    dt1[...] = (wcol[:, 1:2] == lane).astype(F32).astype(BF16)

    blk[...] = jnp.zeros_like(blk)
    wait_for(mbuf.at[0:15], mr.at[0])
    for j in range(16):
        part = mbuf[j]
        blk[128 * j : 128 * j + 64, 0:128] = part
        blk[128 * j + 64 : 128 * j + 128, 128:256] = part
    wait_for(gbuf.at[0:15], gr.at[0])
    branch = jnp.dot(jnp.concatenate([gbuf[j] for j in range(16)], axis=1), blk[...], preferred_element_type=F32)
    hid[0:128, :] = stream[0:128, :].astype(F32) + branch[:, 0:128]
    hid[128:256, :] = stream[128:256, :].astype(F32) + branch[:, 128:256]
    scaled = (hid[...] * gain_ref[pl.ds(t, 1), :]).astype(BF16)
    sent[...] = jnp.dot(dmat[...], scaled, preferred_element_type=F32).reshape(NS, CAP, W).astype(BF16)

    x_all[0, y, x, 0] = sent[s]
    for i, r in enumerate(ORDER):
        for dc in range(2):
            if r == 0 and dc == 0:
                continue
            e = along_z(-r, dc)
            remote(sent.at[e], x_all.at[2 * i // BLOCKS, y, x, 2 * i % BLOCKS + dc], zs.at[0], zr.at[2 * i // BLOCKS], (e, t))

    def span(col, start, size):
        return pl.ds(HALF * col + start, size)

    def by_first(col, ref, k, f, start=0, size=HALF):
        return ref.at[k, :, f, span(col, start, size)] if col == 0 else ref.at[k, f, :, span(col, start, size)]

    def by_second(col, ref, k, g, start=0, size=4):
        fs = pl.ds(start, size)
        return ref.at[k, g, fs, span(col, 0, HALF)] if col == 0 else ref.at[k, fs, g, span(col, 0, HALF)]

    first_of = (x, y)
    second_of = (y, x)

    def on_first(col, f):
        return plane(y, f) if col == 0 else plane(f, x)

    def on_second(col, g):
        return plane(g, x) if col == 0 else plane(y, g)

    inv_gain = 1.0 / (gain_ref[...] * gain_ref[...])

    def gather_first(k):
        wait_for(sent.at[0 : BLOCKS if k else BLOCKS - 1], zr.at[k])
        for col in range(2):
            own = x_all.at[k, y, x, span(col, 0, HALF)]
            for d in (1, 3, 2):
                remote(own, own, ss.at[0], sr.at[0, k], on_first(col, (first_of[col] + d) % 4))

    def gather_second(k):
        wait_for(x_all.at[0, 0, 0:3], sr.at[0, k])
        for col in range(2):
            g = second_of[col]
            for d in (1, 3):
                ref = by_second(col, x_all, k, g)
                remote(ref, ref, ss.at[1], sr.at[1, k], on_second(col, (g + d) % 4))

    def gather_third(k):
        wait_for(x_all.at[0, 0:2], sr.at[1, k])
        for col in range(2):
            g = second_of[col]
            for way, d in enumerate((1, 3)):
                ref = by_second(col, x_all, k, (g + 4 - d) % 4, 2 * way, 2)
                remote(ref, ref, ss.at[2], sr.at[2, k], on_second(col, (g + d) % 4))

    def experts(k):
        wait_for(x_all.at[0, 0], sr.at[2, k])
        squares = jnp.zeros((ROWS, W), F32)
        for j in range(16):
            part = x_all[k, j // 4, j % 4].astype(F32).reshape(ROWS, W)
            squares = squares + part * part * inv_gain[j : j + 1, :]
            lhs[:, W * j : W * (j + 1)] = part.astype(BF16)
        scale = lax.rsqrt(jnp.sum(squares, axis=1, keepdims=True) / 2048.0 + 1e-06)
        gate = jnp.dot(lhs[...], wg[...], preferred_element_type=F32) * scale
        upper = jnp.dot(lhs[...], wu[...], preferred_element_type=F32) * scale
        act = (gate / (1.0 + jnp.exp(-gate)) * upper).astype(BF16)
        for yy in range(4):
            partial = jnp.dot(act, wd[:, 512 * yy : 512 * (yy + 1)], preferred_element_type=F32)
            for xx in range(4):
                p_all[k, yy, xx] = partial[:, W * xx : W * (xx + 1)].reshape(BLOCKS, CAP, W).astype(BF16)
        for col in range(2):
            f = first_of[col]
            for way, d in enumerate((1, 3)):
                ref = by_first(col, p_all, k, (f + 2) % 4, PART * way, PART)
                remote(ref, rb0.at[k, col, way], ss.at[3], sr.at[3, k], on_first(col, (f + d) % 4))

    def reduce_first(k):
        wait_for(x_all.at[0, 0], sr.at[3, k])
        for col in range(2):
            f = first_of[col]
            for way, d in enumerate((1, 3)):
                other = (f + d) % 4
                half = by_first(col, p_all, k, other, PART * way, PART)
                half[...] = (half[...].astype(F32) + rb0[k, col, way].astype(F32)).astype(BF16)
                remote(by_first(col, p_all, k, other), rb1.at[k, col, way], ss.at[4], sr.at[4, k], on_first(col, other))

    def reduce_second(k):
        wait_for(x_all.at[0, 0:2], sr.at[4, k])
        for col in range(2):
            f, g = first_of[col], second_of[col]
            total = by_first(col, p_all, k, f)[...].astype(F32) + rb1[k, col, 0].astype(F32) + rb1[k, col, 1].astype(F32)
            q_all[k, col] = total.astype(BF16)
            for d in (1, 3, 2):
                other = (g + d) % 4
                remote(q_all.at[k, col, other], rb2.at[k, col, d - 1], ss.at[5], sr.at[5, k], on_second(col, other))

    def give_back(k):
        wait_for(x_all.at[0, 0, 0:3], sr.at[5, k])
        for col in range(2):
            total = q_all[k, col, second_of[col]].astype(F32)
            for d in range(3):
                total = total + rb2[k, col, d].astype(F32)
            f_all[k, HALF * col : HALF * (col + 1)] = total.astype(BF16)
        for b in range(BLOCKS):
            i = BLOCKS * k + b
            if i == 0:
                back[s] = f_all[0, 0]
                continue
            home = along_z(ORDER[i // 2], i % 2)
            remote(f_all.at[k, b], back.at[s], bs.at[0], br.at[0], (home, t))

    stages = (gather_first, gather_second, gather_third, experts, reduce_first, reduce_second, give_back)
    for number, k in SCHEDULE:
        stages[number](k)

    wait_for(sent.at[0:31], br.at[0])
    landed = back[...].astype(F32).reshape(NS * CAP, W).astype(BF16)
    one = jnp.dot(dt0[...], landed, preferred_element_type=F32)
    two = jnp.dot(dt1[...], landed, preferred_element_type=F32)
    out_ref[...] = (hid[...] + (wcol[:, 2:3] * one + wcol[:, 3:4] * two)).astype(BF16)
    wait_for(hrecv, hs.at[0])
    wait_for(mbuf.at[0:15], ms.at[0])
    wait_for(gbuf.at[0:15], gs.at[0])
    wait_for(sent.at[0:31], zs.at[0])
    wait_for(sent.at[0:31], bs.at[0])
    for i, size in enumerate((3, 8, 4, 4, 8, 3)):
        wait_for(x_all.at[:, 0 : max(1, size // 4), 0 : min(size, 4)], ss.at[i])


def body(outer_gate, inner_gate, values, conv_taps, document, mix_proj, stream, norm_gain, routes, route_weight, w_gate, w_up, w_down):
    vmem = pl.BlockSpec(memory_space=pltpu.VMEM)
    hbm = pl.BlockSpec(memory_space=pl.ANY)
    dma = pltpu.SemaphoreType.DMA
    scratch = [
        pltpu.VMEM((3, 64, 256), BF16),
        pltpu.VMEM((3, 64), BF16),
        pltpu.VMEM((1, 256), jnp.int32),
        pltpu.VMEM((16, 128), F32),
        pltpu.VMEM((2, 256), jnp.int32),
        pltpu.VMEM((2, 256), F32),
        pltpu.VMEM((64, 2048), BF16),
        pltpu.VMEM((256, W), BF16),
        pltpu.VMEM((2048, 256), BF16),
        pltpu.VMEM((2048, 256), BF16),
        pltpu.VMEM((256, 2048), BF16),
        pltpu.VMEM((72, 128), F32),
        pltpu.VMEM((72, 128), F32),
        pltpu.VMEM((16, 64, W), BF16),
        pltpu.VMEM((2048, 256), BF16),
        pltpu.VMEM((16, 128, 128), BF16),
        pltpu.VMEM((256, W), F32),
        pltpu.VMEM((NS * CAP, 256), BF16),
        pltpu.VMEM((256, NS * CAP), BF16),
        pltpu.VMEM((256, NS * CAP), BF16),
        pltpu.VMEM((256, 128), F32),
        pltpu.VMEM((NS, CAP, W), BF16),
        pltpu.VMEM((CHUNKS, 4, 4, BLOCKS, CAP, W), BF16),
        pltpu.VMEM((ROWS, 2048), BF16),
        pltpu.VMEM((CHUNKS, 4, 4, BLOCKS, CAP, W), BF16),
        pltpu.VMEM((CHUNKS, 2, 2, 4, PART, CAP, W), BF16),
        pltpu.VMEM((CHUNKS, 2, 2, 4, HALF, CAP, W), BF16),
        pltpu.VMEM((CHUNKS, 2, 3, HALF, CAP, W), BF16),
        pltpu.VMEM((CHUNKS, 2, 4, HALF, CAP, W), BF16),
        pltpu.VMEM((CHUNKS, BLOCKS, CAP, W), BF16),
        pltpu.VMEM((NS, CAP, W), BF16),
        dma((13,)),
        dma((1,)), dma((1,)),
        dma((1,)), dma((1,)),
        dma((1,)), dma((1,)),
        dma((1,)), dma((CHUNKS,)),
        dma((6,)), dma((6, CHUNKS)),
        dma((1,)), dma((1,)),
    ]
    return pl.pallas_call(
        kernel,
        out_shape=jax.ShapeDtypeStruct((256, W), BF16),
        in_specs=[hbm] * 13,
        out_specs=vmem,
        scratch_shapes=scratch,
        compiler_params=pltpu.CompilerParams(collective_id=0, has_side_effects=True, vmem_limit_bytes=60 * 2**20),
        name="block",
    )(
        outer_gate.T, inner_gate.T, values.T, conv_taps, document.reshape(1, 256), mix_proj, stream, norm_gain.reshape(16, 128),
        routes.T, route_weight.T, w_gate[0], w_up[0], w_down[0],
    )


def solution(mesh):
    placed = (
        P("sp", "tp"), P("sp", "tp"), P("sp", "tp"), P(None, "tp"), P("sp"), P("tp", None), P("sp", None), P(),
        P("sp", None), P("sp", None), P("sp", None, "tp"), P("sp", None, "tp"), P("sp", "tp", None),
    )
    return jax.shard_map(body, mesh=mesh, in_specs=placed, out_specs=P("sp", "tp"), check_vma=False)
```

time: 90.4 us -> 84.3 us (0.933)
  Pallas kernels: 88.7 us -> 82.7 us
    pallas_call x1, Pallas kernels: 88.7 us -> 82.7 us  [body(): pl.pallas_call(kernel, out_shape=jax.ShapeDtypeStruct((256, W), BF16), in...]
where the time goes in v2:
time: 84.3 us; the launch traced here: 84.2 us
  Pallas kernels  82.7 us (98%)
  local copies, waits for them, and re-layouts  1.47 us (2%)
    pallas_call x1, Pallas kernels, body(): pl.pallas_call(kernel, out_shape=jax.ShapeDtypeStruct((256, W), BF16), in...  82.7 us

profile of v2, /device:TPU:1, one launch (start us, length us, event | category | flops | bytes accessed | tf_op | source)
XLA Modules:
  0.0 84.2 jit_solution(5509901734169848206)
XLA Ops:
  0.0 82.7 %block.1 = bf16[256,128]{1,0:T(8,128)(2,1)} custom-call(bf16[64,256]{1,0:T(8,128)(2,1)} %bitcast.13, bf16[64,256]{1,0:T(8,128)(2,1)} %bitcast.14, bf16[64,256]{1,0:T(8,128)(2,1)} %bitcast.15, bf16[3,64]{1,0:T(4,128)(2,1)} %taps_hbm.1, s32[1,256]{1,0:T(1,128)} %bitcast.19, bf16[64,2048]{1,0:T(8,128)(2,1)} %mix_hbm.1, bf16[256,2048]{1,0:T(8,128)(2,1)} %stream_hbm.1, ...), custom_call_target="tpu_custom_call" | custom-call | tf_op jit(solution)/shard_map/block/pallas_call | solution.py:307
  82.7 1.5 %copy.15 = bf16[256,128]{1,0:T(8,128)(2,1)} copy(bf16[256,128]{1,0:T(8,128)(2,1)} %block.1) | data formatting | bytes 131072

commit v3 on v2

--- a/solution.py
+++ b/solution.py
@@ -21,7 +21,7 @@
 
 ORDER = (0, 1, 14, 3, 13, 4, 9, 8, 10, 7, 11, 6, 12, 5, 15, 2)
 
-SCHEDULE = ((0, 0), (0, 1), (0, 2), (1, 0), (1, 1), (1, 2), (0, 3), (2, 0), (0, 4), (0, 7), (0, 5), (2, 1), (2, 2), (0, 6), (1, 3), (1, 4), (1, 5), (1, 7), (2, 3), (3, 2), (2, 4), (1, 6), (2, 5), (3, 1), (2, 7), (3, 3), (4, 2), (3, 4), (2, 6), (3, 0), (3, 5), (3, 7), (4, 3), (4, 4), (3, 6), (4, 7), (5, 3), (4, 5), (5, 4), (4, 6), (4, 1), (5, 5), (4, 0), (6, 3), (6, 4), (5, 6), (5, 2), (5, 7), (5, 1), (6, 5), (5, 0), (6, 6), (6, 2), (6, 1), (6, 7), (6, 0))
+SCHEDULE = ((0, 0), (0, 1), (1, 0), (0, 2), (1, 1), (0, 3), (0, 7), (0, 5), (0, 6), (0, 4), (1, 2), (2, 1), (1, 3), (1, 5), (1, 4), (1, 6), (2, 3), (3, 1), (2, 5), (2, 0), (2, 4), (1, 7), (2, 6), (3, 3), (2, 2), (4, 1), (3, 5), (3, 4), (2, 7), (4, 3), (3, 6), (3, 2), (4, 5), (4, 4), (5, 3), (5, 1), (3, 7), (4, 6), (3, 0), (5, 4), (4, 2), (5, 5), (6, 3), (4, 7), (5, 6), (6, 1), (4, 0), (6, 4), (5, 2), (6, 5), (5, 7), (5, 0), (6, 6), (6, 2), (6, 7), (6, 0))
 
 NT = (((1,), (1,)), ((), ()))
 
@@ -29,8 +29,8 @@
 def kernel(
     og_hbm, ig_hbm, vv_hbm, taps_hbm, doc_hbm, mix_hbm, stream_hbm, gain_hbm, routes_hbm, rw_hbm, wg_hbm, wu_hbm, wd_hbm,
     out_ref,
-    gates, taps_ref, doc_ref, gain_ref, routes_ref, rw_ref, mix, stream, wg, wu, wd, hsend, hrecv, mbuf, blk, gbuf, hid, dmat, dt0, dt1, wcol, sent, x_all, lhs, p_all, rb0, rb1, rb2, q_all, f_all, back,
-    lsem, hs, hr, ms, mr, gs, gr, zs, zr, ss, sr, bs, br,
+    gates, taps_ref, doc_ref, gain_ref, routes_ref, rw_ref, mix, stream, wg, wu, wd, hsend, hrecv, mbuf, mother, gfix, blk, gbuf, hid, dmat, dt0, dt1, wcol, sent, x_all, lhs, p_all, rb0, rb1, rb2, q_all, f_all, back,
+    lsem, hs, hr, ms, mr, gs, gr, fs, fr, zs, zr, ss, sr, bs, br,
 ):
     s = lax.axis_index("sp")
     t = lax.axis_index("tp")
@@ -50,7 +50,7 @@
         pl.semaphore_signal(barrier, inc=1, device_id=((s + d) % NS, t), device_id_type=MESH)
 
     pairs = (
-        (ig_hbm, gates.at[0]), (vv_hbm, gates.at[1]), (doc_hbm, doc_ref), (mix_hbm, mix), (og_hbm, gates.at[2]), (taps_hbm, taps_ref),
+        (ig_hbm, gates.at[0]), (vv_hbm, gates.at[1]), (doc_hbm, doc_ref), (og_hbm, gates.at[2]), (taps_hbm, taps_ref), (mix_hbm, mix),
         (routes_hbm, routes_ref), (rw_hbm, rw_ref), (gain_hbm, gain_ref),
         (stream_hbm.at[:, pl.ds(pl.multiple_of(t * W, W), W)], stream), (wg_hbm, wg), (wu_hbm, wu), (wd_hbm, wd),
     )
@@ -67,41 +67,45 @@
         )
         copy.start()
 
-    for load in loads[:3]:
+    for load in loads[:6]:
         load.wait()
     product = gates[0].astype(F32) * gates[1].astype(F32)
     doc = jnp.broadcast_to(doc_ref[...].astype(F32), (8, 256))
     hsend[0:64, :] = product[:, 128:]
     hsend[64:72, :] = doc[:, 128:]
-    loads[3].wait()
+    eye = (lax.broadcasted_iota(jnp.int32, (64, 64), 0) == lax.broadcasted_iota(jnp.int32, (64, 64), 1)).astype(BF16)
+    kernel_taps = lax.dot_general(eye, taps_ref[...], NT, preferred_element_type=F32)
+
+    def convolve(before, doc_before):
+        long = jnp.concatenate([before, product], axis=1)
+        long_doc = jnp.concatenate([doc_before, doc], axis=1)
+        conv = kernel_taps[:, 2:3] * product
+        for step in (1, 2):
+            shifted = pltpu.roll(long, step, 1)[:, 128:]
+            same = (pltpu.roll(long_doc, step, 1)[:, 128:] == doc)[0:1, :]
+            conv = conv + kernel_taps[:, 2 - step : 3 - step] * jnp.where(same, shifted, 0.0)
+        gated = gates[2].astype(F32) * conv
+        return jnp.concatenate([gated[:, :128], gated[:, 128:]], axis=0).T.astype(BF16)
+
+    gbuf[t] = convolve(jnp.zeros((64, 128), F32), jnp.full((8, 128), -1.0, F32))
     pl.semaphore_wait(barrier, 15 + NS - 1)
 
     remote(hsend, hrecv, hs.at[0], hr.at[0], ((s + 1) % NS, t))
+    half_rows = pl.ds(pl.multiple_of(16 * (2 * (z % 2) + c), 16), 16)
     for d in range(1, 16):
         j = (t + d) % 16
-        remote(mix.at[:, pl.ds(pl.multiple_of(j * W, W), W)], mbuf.at[t], ms.at[0], mr.at[0], (s, j))
-    mbuf[t] = mix[:, pl.ds(pl.multiple_of(t * W, W), W)]
-
-    eye = (lax.broadcasted_iota(jnp.int32, (64, 64), 0) == lax.broadcasted_iota(jnp.int32, (64, 64), 1)).astype(BF16)
-    for load in loads[4:]:
-        load.wait()
-    kernel_taps = lax.dot_general(eye, taps_ref[...], NT, preferred_element_type=F32)
-
-    wait_for(hrecv, hr.at[0])
-    before = hrecv[0:64, :]
-    doc_before = jnp.where(s == 0, -1.0, hrecv[64:72, :])
-    long = jnp.concatenate([before, product], axis=1)
-    long_doc = jnp.concatenate([doc_before, doc], axis=1)
-    conv = kernel_taps[:, 2:3] * product
-    for step in (1, 2):
-        shifted = pltpu.roll(long, step, 1)[:, 128:]
-        same = (pltpu.roll(long_doc, step, 1)[:, 128:] == doc)[0:1, :]
-        conv = conv + kernel_taps[:, 2 - step : 3 - step] * jnp.where(same, shifted, 0.0)
-    gated = gates[2].astype(F32) * conv
-    folded = jnp.concatenate([gated[:, :128], gated[:, 128:]], axis=0)
-    gbuf[t] = folded.T.astype(BF16)
+        remote(mix.at[half_rows, pl.ds(pl.multiple_of(j * W, W), W)], mbuf.at[t], ms.at[0], mr.at[0], (s, j))
     for d in range(1, 16):
         remote(gbuf.at[t], gbuf.at[t], gs.at[0], gr.at[0], (s, (t + d) % 16))
+    mbuf[t] = mix[half_rows, pl.ds(pl.multiple_of(t * W, W), W)]
+    for load in loads[6:]:
+        load.wait()
+
+    wait_for(hrecv, hr.at[0])
+    folded = convolve(hrecv[0:64, :], jnp.where(s == 0, -1.0, hrecv[64:72, :]))
+    gfix[t] = folded[0:8, :]
+    for d in range(1, 16):
+        remote(gfix.at[t], gfix.at[t], fs.at[0], fr.at[0], (s, (t + d) % 16))
 
     expert = lax.broadcasted_iota(jnp.int32, (NS, 256), 0)
     first = (routes_ref[0:1, :] == expert).astype(F32)
@@ -123,14 +127,32 @@
 
     blk[...] = jnp.zeros_like(blk)
     wait_for(mbuf.at[0:15], mr.at[0])
-    for j in range(16):
-        part = mbuf[j]
-        blk[128 * j : 128 * j + 64, 0:128] = part
-        blk[128 * j + 64 : 128 * j + 128, 128:256] = part
+    remote(mbuf, mother.at[0], ms.at[1], mr.at[1], (s + 2 - 4 * (z % 2), t))
+
+    def spread(buffer, quarter):
+        for j in range(16):
+            part = buffer[j]
+            blk[pl.ds(pl.multiple_of(128 * j + 16 * quarter, 16), 16), 0:128] = part
+            blk[pl.ds(pl.multiple_of(128 * j + 64 + 16 * quarter, 16), 16), 128:256] = part
+
+    odd = z % 2
+    spread(mbuf, 2 * odd + c)
+    wait_for(mother.at[0], mr.at[1])
+    remote(mbuf, mother.at[1], ms.at[2], mr.at[2], (s + 1 - 2 * c, t))
+    remote(mother.at[0], mother.at[2], ms.at[3], mr.at[3], (s + 1 - 2 * c, t))
+    spread(mother.at[0], 2 - 2 * odd + c)
+    wait_for(mother.at[1], mr.at[2])
+    spread(mother.at[1], 2 * odd + 1 - c)
+    wait_for(mother.at[2], mr.at[3])
+    spread(mother.at[2], 3 - 2 * odd - c)
     wait_for(gbuf.at[0:15], gr.at[0])
     branch = jnp.dot(jnp.concatenate([gbuf[j] for j in range(16)], axis=1), blk[...], preferred_element_type=F32)
-    hid[0:128, :] = stream[0:128, :].astype(F32) + branch[:, 0:128]
+    hid[8:128, :] = stream[8:128, :].astype(F32) + branch[8:128, 0:128]
     hid[128:256, :] = stream[128:256, :].astype(F32) + branch[:, 128:256]
+    wait_for(gfix.at[0:15], fr.at[0])
+    fixed = jnp.concatenate([gfix[j].astype(F32) for j in range(16)], axis=1).astype(BF16)
+    branch = jnp.dot(fixed, blk[...], preferred_element_type=F32)
+    hid[0:8, :] = stream[0:8, :].astype(F32) + branch[:, 0:128]
     scaled = (hid[...] * gain_ref[pl.ds(t, 1), :]).astype(BF16)
     sent[...] = jnp.dot(dmat[...], scaled, preferred_element_type=F32).reshape(NS, CAP, W).astype(BF16)
 
@@ -253,6 +275,9 @@
     out_ref[...] = (hid[...] + (wcol[:, 2:3] * one + wcol[:, 3:4] * two)).astype(BF16)
     wait_for(hrecv, hs.at[0])
     wait_for(mbuf.at[0:15], ms.at[0])
+    for i in range(1, 4):
+        wait_for(mbuf, ms.at[i])
+    wait_for(gfix.at[0:15], fs.at[0])
     wait_for(gbuf.at[0:15], gs.at[0])
     wait_for(sent.at[0:31], zs.at[0])
     wait_for(sent.at[0:31], bs.at[0])
@@ -278,7 +303,9 @@
         pltpu.VMEM((256, 2048), BF16),
         pltpu.VMEM((72, 128), F32),
         pltpu.VMEM((72, 128), F32),
-        pltpu.VMEM((16, 64, W), BF16),
+        pltpu.VMEM((16, 16, W), BF16),
+        pltpu.VMEM((3, 16, 16, W), BF16),
+        pltpu.VMEM((16, 8, W), BF16),
         pltpu.VMEM((2048, 256), BF16),
         pltpu.VMEM((16, 128, 128), BF16),
         pltpu.VMEM((256, W), F32),
@@ -298,6 +325,7 @@
         pltpu.VMEM((NS, CAP, W), BF16),
         dma((13,)),
         dma((1,)), dma((1,)),
+        dma((4,)), dma((4,)),
         dma((1,)), dma((1,)),
         dma((1,)), dma((1,)),
         dma((1,)), dma((CHUNKS,)),

time: 84.3 us -> 83.2 us (0.987)
  Pallas kernels: 82.7 us -> 81.5 us
    pallas_call x1, Pallas kernels: 82.7 us -> 81.5 us  [body(): pl.pallas_call(kernel, out_shape=jax.ShapeDtypeStruct((256, W), BF16), in...]
where the time goes in v3:
time: 83.2 us; the launch traced here: 83 us
  Pallas kernels  81.5 us (98%)
  local copies, waits for them, and re-layouts  1.47 us (2%)
    pallas_call x1, Pallas kernels, body(): pl.pallas_call(kernel, out_shape=jax.ShapeDtypeStruct((256, W), BF16), in...  81.5 us

profile of v3, /device:TPU:1, one launch (start us, length us, event | category | flops | bytes accessed | tf_op | source)
XLA Modules:
  0.0 83.0 jit_solution(8165712652067353812)
XLA Ops:
  0.0 81.5 %block.1 = bf16[256,128]{1,0:T(8,128)(2,1)} custom-call(bf16[64,256]{1,0:T(8,128)(2,1)} %bitcast.13, bf16[64,256]{1,0:T(8,128)(2,1)} %bitcast.14, bf16[64,256]{1,0:T(8,128)(2,1)} %bitcast.15, bf16[3,64]{1,0:T(4,128)(2,1)} %taps_hbm.1, s32[1,256]{1,0:T(1,128)} %bitcast.19, bf16[64,2048]{1,0:T(8,128)(2,1)} %mix_hbm.1, bf16[256,2048]{1,0:T(8,128)(2,1)} %stream_hbm.1, ...), custom_call_target="tpu_custom_call" | custom-call | tf_op jit(solution)/shard_map/block/pallas_call | solution.py:335
  81.5 1.5 %copy.15 = bf16[256,128]{1,0:T(8,128)(2,1)} copy(bf16[256,128]{1,0:T(8,128)(2,1)} %block.1) | data formatting | bytes 131072

commit v4 on v3

--- a/solution.py
+++ b/solution.py
@@ -22,6 +22,8 @@
 ORDER = (0, 1, 14, 3, 13, 4, 9, 8, 10, 7, 11, 6, 12, 5, 15, 2)
 
 SCHEDULE = ((0, 0), (0, 1), (1, 0), (0, 2), (1, 1), (0, 3), (0, 7), (0, 5), (0, 6), (0, 4), (1, 2), (2, 1), (1, 3), (1, 5), (1, 4), (1, 6), (2, 3), (3, 1), (2, 5), (2, 0), (2, 4), (1, 7), (2, 6), (3, 3), (2, 2), (4, 1), (3, 5), (3, 4), (2, 7), (4, 3), (3, 6), (3, 2), (4, 5), (4, 4), (5, 3), (5, 1), (3, 7), (4, 6), (3, 0), (5, 4), (4, 2), (5, 5), (6, 3), (4, 7), (5, 6), (6, 1), (4, 0), (6, 4), (5, 2), (6, 5), (5, 7), (5, 0), (6, 6), (6, 2), (6, 7), (6, 0))
+
+FAR_FIRST = sorted(((dy, dx) for dy in range(4) for dx in range(4) if dy or dx), key=lambda d: -min(d[0], 4 - d[0]) - min(d[1], 4 - d[1]))
 
 NT = (((1,), (1,)), ((), ()))
 
@@ -91,12 +93,12 @@
     pl.semaphore_wait(barrier, 15 + NS - 1)
 
     remote(hsend, hrecv, hs.at[0], hr.at[0], ((s + 1) % NS, t))
+    others = [(y + dy) % 4 * 4 + (x + dx) % 4 for dy, dx in FAR_FIRST]
     half_rows = pl.ds(pl.multiple_of(16 * (2 * (z % 2) + c), 16), 16)
-    for d in range(1, 16):
-        j = (t + d) % 16
+    for j in others:
         remote(mix.at[half_rows, pl.ds(pl.multiple_of(j * W, W), W)], mbuf.at[t], ms.at[0], mr.at[0], (s, j))
-    for d in range(1, 16):
-        remote(gbuf.at[t], gbuf.at[t], gs.at[0], gr.at[0], (s, (t + d) % 16))
+    for j in others:
+        remote(gbuf.at[t], gbuf.at[t], gs.at[0], gr.at[0], (s, j))
     mbuf[t] = mix[half_rows, pl.ds(pl.multiple_of(t * W, W), W)]
     for load in loads[6:]:
         load.wait()
@@ -104,8 +106,8 @@
     wait_for(hrecv, hr.at[0])
     folded = convolve(hrecv[0:64, :], jnp.where(s == 0, -1.0, hrecv[64:72, :]))
     gfix[t] = folded[0:8, :]
-    for d in range(1, 16):
-        remote(gfix.at[t], gfix.at[t], fs.at[0], fr.at[0], (s, (t + d) % 16))
+    for j in others:
+        remote(gfix.at[t], gfix.at[t], fs.at[0], fr.at[0], (s, j))
 
     expert = lax.broadcasted_iota(jnp.int32, (NS, 256), 0)
     first = (routes_ref[0:1, :] == expert).astype(F32)

time: 83.2 us -> 85.2 us (1.024)
  Pallas kernels: 81.5 us -> 83.5 us
    pallas_call x1, Pallas kernels: 81.5 us -> 83.5 us  [body(): pl.pallas_call(kernel, out_shape=jax.ShapeDtypeStruct((256, W), BF16), in...]
where the time goes in v4:
time: 85.2 us; the launch traced here: 85 us
  Pallas kernels  83.5 us (98%)
  local copies, waits for them, and re-layouts  1.47 us (2%)
    pallas_call x1, Pallas kernels, body(): pl.pallas_call(kernel, out_shape=jax.ShapeDtypeStruct((256, W), BF16), in...  83.5 us

profile of v4, /device:TPU:1, one launch (start us, length us, event | category | flops | bytes accessed | tf_op | source)
XLA Modules:
  0.0 85.0 jit_solution(2980696114701343678)
XLA Ops:
  0.0 83.5 %block.1 = bf16[256,128]{1,0:T(8,128)(2,1)} custom-call(bf16[64,256]{1,0:T(8,128)(2,1)} %bitcast.13, bf16[64,256]{1,0:T(8,128)(2,1)} %bitcast.14, bf16[64,256]{1,0:T(8,128)(2,1)} %bitcast.15, bf16[3,64]{1,0:T(4,128)(2,1)} %taps_hbm.1, s32[1,256]{1,0:T(1,128)} %bitcast.19, bf16[64,2048]{1,0:T(8,128)(2,1)} %mix_hbm.1, bf16[256,2048]{1,0:T(8,128)(2,1)} %stream_hbm.1, ...), custom_call_target="tpu_custom_call" | custom-call | tf_op jit(solution)/shard_map/block/pallas_call | solution.py:337
  83.5 1.5 %copy.15 = bf16[256,128]{1,0:T(8,128)(2,1)} copy(bf16[256,128]{1,0:T(8,128)(2,1)} %block.1) | data formatting | bytes 131072
